TPU v7x, 32 devices: a whole 2x2x4 slice. The times are simulated.
32 devices in a mesh: grp: 2 (over y), fs: 4 (over z), tp: 4 (over x, core).
Axes of the slice: x: 2, y: 2, z: 4, core: 2. Of those that a mesh axis runs over, the one named last changes fastest.
Arguments:
- tokens: bfloat16 [2048, 3072], P(('grp', 'tp')), parts along dimension 0, may hold values from -6 to 6
- up_master: float32 [3072, 12288], P('fs', 'tp'), may hold values from -0.109375 to 0.109375
- down_master: float32 [12288, 3072], P('fs', 'tp'), may hold values from -0.0546875 to 0.0546875
- norm_gain: float32 [3072], P('fs'), may hold values from 0.1 to 1.9
Outputs:
- prompt_out: bfloat16 [2048, 3072], P(('grp', 'tp'), 'fs'), parts along dimension 0
- sampled_up: bfloat16 [6144, 12288], P('grp', 'fs'), parts along dimension 0
- sampled_down: bfloat16 [24576, 3072], P(('grp', 'fs')), parts along dimension 0
There are 2 independent parts, one for each index of `grp`. A program takes and returns all parts, laid end to end along the dimension named above; an argument that names none is the same for every part. Nothing has to cross between parts.
All inputs are finite; a program needn't handle non-finite values.
Results may differ from a plain program's by a relative error of at most 0.0074.
Values may be sent and summed in bfloat16 or wider, within the bound.
A program may use at most 192 MiB of HBM per device.

v0:
```python
import jax
import jax.numpy as jnp
from jax import lax
from jax.sharding import PartitionSpec as P


def normalize(tokens):
    values = tokens.astype(jnp.float32)
    center = jnp.mean(values, axis=-1, keepdims=True)
    spread = jnp.mean(jnp.square(values - center), axis=-1, keepdims=True)
    return ((values - center) * lax.rsqrt(spread + 1e-05)).astype(jnp.bfloat16)


def shards(tokens, up_master, down_master, norm_gain):
    up_cast = (norm_gain[:, None] * up_master).astype(jnp.bfloat16)
    down_cast = down_master.astype(jnp.bfloat16)
    quarter = lax.all_to_all(up_cast, "tp", split_axis=0, concat_axis=1, tiled=True)
    moved = lax.all_to_all(quarter, "fs", split_axis=1, concat_axis=0, tiled=True)
    part_rows = quarter.shape[0]
    stacked = moved.reshape(moved.shape[0] // part_rows, part_rows, moved.shape[1])
    joined, sampled_down = (
        lax.all_gather(stacked, "tp", axis=1, tiled=True),
        lax.all_gather(down_cast, "tp", axis=1, tiled=True),
    )
    sampled_up = joined.reshape(joined.shape[0] * joined.shape[1], joined.shape[2])
    normalized = normalize(tokens)
    before = jnp.dot(normalized, sampled_up, preferred_element_type=jnp.float32)
    hidden = jnp.square(jax.nn.relu(before)).astype(jnp.bfloat16)
    terms = jnp.dot(hidden, sampled_down, preferred_element_type=jnp.float32)
    summed = lax.psum_scatter(terms, "fs", scatter_dimension=1, tiled=True)
    return (summed.astype(jnp.bfloat16), sampled_up, sampled_down)


def solution(mesh):
    return jax.shard_map(
        shards,
        mesh=mesh,
        in_specs=(P(("grp", "tp"), None), P("fs", "tp"), P("fs", "tp"), P("fs")),
        out_specs=(P(("grp", "tp"), "fs"), P("grp", "fs"), P(("grp", "fs"), None)),
        check_vma=False,
    )
```

profile of v0, /device:TPU:3, one launch (start us, length us, event | category | flops | bytes accessed | tf_op | source)
XLA Modules:
  0.0 523.1 jit_solution(6429137152449388254)
XLA Ops:
  7.2 0.0 all-gather.3.cloned.1.call-start
  7.2 5.1 multiply_convert_fusion
  12.3 55.3 %all_to_all.29 = bf16[4,192,3072]{2,1,0:T(8,128)(2,1)S(1)} all-to-all(bf16[4,192,3072]{2,1,0:T(8,128)(2,1)S(1)} %bitcast.13), channel_id=1, replica_groups=mesh['grp'=2,'fs'=4,'tp'=4] {'tp'}, dimensions={0} | all-to-all | bytes 9437184 | tf_op jit(solution)/shard_map/all_to_all | solution.py:17
  67.6 108.4 %all_to_all.30 = bf16[192,4,3072]{2,0,1:T(8,128)(2,1)} all-to-all(bf16[192,4,3072]{2,0,1:T(8,128)(2,1)S(1)} %bitcast.12), channel_id=1, replica_groups=mesh['grp'=2,'fs'=4,'tp'=4] {'fs'}, dimensions={1} | all-to-all | bytes 9437184 | tf_op jit(solution)/shard_map/all_to_all | solution.py:18
  176.0 0.0 all-gather.3.cloned.1.call-update
  176.1 0.0 all-gather.5.cloned.1.call-start
  176.1 6.3 %convert_element_type.22 = bf16[3072,768]{1,0:T(8,128)(2,1)} convert(f32[3072,768]{1,0:T(8,128)} %param.6) | non-fusion elementwise | flops 2359296 | bytes 14155776 | tf_op jit(solution)/shard_map/convert_element_type | solution.py:16
  182.4 0.0 copy-start
  182.4 0.0 all-gather.5.cloned.1.call-update
  182.5 0.0 reduce-scatter.2.cloned.1.call-start
  182.5 1.6 copy-done
  184.1 0.3 convert_reduce_fusion
  184.4 0.6 fusion.4
  185.0 109.8 %all-gather.3.cloned.1.call-done = bf16[4,768,3072]{2,1,0:T(8,128)(2,1)} async-done(((bf16[4,192,3072]{2,1,0:T(8,128)(2,1)}), bf16[4,768,3072]{2,1,0:T(8,128)(2,1)}) %all-gather.3.cloned.1.call-update) | async-done | bytes 18874384 | tf_op jit(solution)/shard_map/all_gather | solution.py:22
  294.8 9.4 %fusion.1 = bf16[256,3072]{1,0:T(8,128)(2,1)S(1)} fusion(bf16[3072,3072]{1,0:T(8,128)(2,1)} %bitcast.7, bf16[256,3072]{1,0:T(8,128)(2,1)S(1)} %copy-done, f32[256]{0:T(256)S(1)} %add_rsqrt_fusion, f32[256]{0:T(256)S(1)} %broadcast_multiply_fusion), kind=kOutput, calls=%fused_computation.5 | convolution fusion | flops 4837343232 | bytes 22022144 | tf_op jit(solution)/shard_map/dot_general | solution.py:27
  304.3 112.7 %all-gather.5.cloned.1.call-done = bf16[3072,3072]{1,0:T(8,128)(2,1)} async-done(((bf16[3072,768]{1,0:T(8,128)(2,1)}), bf16[3072,3072]{1,0:T(8,128)(2,1)}) %all-gather.5.cloned.1.call-update) | async-done | bytes 18874384 | tf_op jit(solution)/shard_map/all_gather | solution.py:23
  417.0 10.7 %fusion.9 = f32[256,3072]{1,0:T(8,128)} fusion(bf16[256,3072]{1,0:T(8,128)(2,1)S(1)} %fusion.1, bf16[3072,3072]{1,0:T(8,128)(2,1)} %all-gather.5.cloned.1.call-done), kind=kOutput, calls=%fused_computation.14 | convolution fusion | flops 4831838208 | bytes 23592960 | tf_op jit(solution)/shard_map/dot_general | solution.py:29
  427.7 0.0 reduce-scatter.2.cloned.1.call-update
  427.7 60.9 %reduce-scatter.2.cloned.1.call-done = f32[256,768]{1,0:T(8,128)} async-done(((f32[256,3072]{1,0:T(8,128)}), f32[256,768]{1,0:T(8,128)}) %reduce-scatter.2.cloned.1.call-update) | async-done | bytes 786448 | tf_op jit(solution)/shard_map/reduce_scatter | solution.py:30
  488.5 0.0 slice-start
  488.6 2.1 convert_element_type.23
  490.6 0.0 slice-start.1
  490.6 0.0 slice-start.2
  490.6 0.0 slice-start.3
  490.6 0.0 slice-start.4
  490.6 19.1 %copy.9 = bf16[3072,3072]{1,0:T(8,128)(2,1)} copy(bf16[3072,3072]{1,0:T(8,128)(2,1)} %bitcast.8) | data formatting | bytes 37748736
  509.7 0.0 slice-done
  509.7 0.0 slice-done.1
  509.7 0.0 slice-done.2
  509.7 0.0 slice-done.3
  509.7 0.0 slice-done.4
  509.8 6.9 %copy.10 = bf16[3072,3072]{1,0:T(8,128)(2,1)} copy(bf16[3072,3072]{1,0:T(8,128)(2,1)S(1)} %bitcast.10) | data formatting | bytes 37748736
  (3 shorter events, 0.0 us)
Async XLA Ops:
  7.2 287.7 %all-gather.3.cloned.1.call-start = ((), (), s32[]{:S(2)}) async-start(), calls=%async_computation.3 | async-start | bytes 23592960 | tf_op jit(solution)/shard_map/all_gather | solution.py:22
  176.1 240.9 %all-gather.5.cloned.1.call-start = ((), (), s32[]{:S(2)}) async-start(), calls=%async_computation.4 | async-start | bytes 23592960 | tf_op jit(solution)/shard_map/all_gather | solution.py:23
  182.4 1.7 copy-start
  182.5 306.1 %reduce-scatter.2.cloned.1.call-start = ((), (), s32[]{:S(2)}) async-start(), calls=%async_computation.5 | async-start | bytes 3932160 | tf_op jit(solution)/shard_map/reduce_scatter | solution.py:30
  488.5 21.2 %slice-start = ((s8[18874368]{0:T(1024)(128)(4,1)}), s8[4194304]{0:T(1024)(128)(4,1)S(1)}, s32[]{:S(2)}) async-start(s8[18874368]{0:T(1024)(128)(4,1)} %bitcast.9), calls=%async_computation.6 | async-start | bytes 8388608
  490.6 19.1 %slice-start.1 = ((s8[18874368]{0:T(1024)(128)(4,1)}), s8[4194304]{0:T(1024)(128)(4,1)S(1)}, s32[]{:S(2)}) async-start(s8[18874368]{0:T(1024)(128)(4,1)} %bitcast.9), calls=%async_computation.7 | async-start | bytes 8388608
  490.6 19.1 %slice-start.2 = ((s8[18874368]{0:T(1024)(128)(4,1)}), s8[4194304]{0:T(1024)(128)(4,1)S(1)}, s32[]{:S(2)}) async-start(s8[18874368]{0:T(1024)(128)(4,1)} %bitcast.9), calls=%async_computation.8 | async-start | bytes 8388608
  490.6 19.1 %slice-start.3 = ((s8[18874368]{0:T(1024)(128)(4,1)}), s8[4194304]{0:T(1024)(128)(4,1)S(1)}, s32[]{:S(2)}) async-start(s8[18874368]{0:T(1024)(128)(4,1)} %bitcast.9), calls=%async_computation.9 | async-start | bytes 8388608
  490.6 19.1 %slice-start.4 = ((s8[18874368]{0:T(1024)(128)(4,1)}), s8[2097152]{0:T(1024)(128)(4,1)S(1)}, s32[]{:S(2)}) async-start(s8[18874368]{0:T(1024)(128)(4,1)} %bitcast.9), calls=%async_computation.10 | async-start | bytes 4194304
Sparse Core Ops, SparseCore 0:
  176.2 118.5 all-gather.2
  297.0 119.9 all-gather.4
  427.8 60.6 reduce-scatter.1
where the time goes:
time: 525 us; the launch traced here: 523 us
  waiting for transfers between devices  283 us (54%)
  blocking collectives  164 us (31%)
  local copies, waits for them, and re-layouts  27.6 us (5%)
  matrix products  20.1 us (4%)
  other arithmetic  14.4 us (3%)
  between operations  13.8 us (3%)
    all_gather x1, waiting for transfers between devices, shards(): lax.all_gather(down_cast, 'tp', axis=1, tiled=True)  113 us
    all_gather x1, waiting for transfers between devices, shards(): lax.all_gather(stacked, 'tp', axis=1, tiled=True)  110 us
    all_to_all x1, blocking collectives, shards(): lax.all_to_all(quarter, 'fs', split_axis=1, concat_axis=0, tiled=True)  108 us
    reduce_scatter x1, waiting for transfers between devices, shards(): summed = lax.psum_scatter(terms, 'fs', scatter_dimension=1, tiled=True)  60.9 us
    all_to_all x1, blocking collectives, shards(): lax.all_to_all(up_cast, 'tp', split_axis=0, concat_axis=1, tiled=True)  55.3 us
    unnamed x14, local copies, waits for them, and re-layouts  27.6 us
    dot_general x1, matrix products, shards(): terms = jnp.dot(hidden, sampled_down, preferred_element_type=jnp.float32)  10.7 us
  transfers between devices with their start and end apart: 3, of which 3 were waited for; matrix products, arithmetic and copies ran while one was open for 3% of the time, Pallas kernels for 0%

commit v1 on v0

v1 whole, which is shorter than its diff:
```python
import functools

import jax
import jax.numpy as jnp
from jax import lax
from jax.experimental import pallas as pl
from jax.experimental.pallas import tpu as pltpu
from jax.sharding import PartitionSpec as P

MESH = pl.DeviceIdType.MESH
CORES = 2
LAG = 2


def normalize(tokens):
    values = tokens.astype(jnp.float32)
    center = jnp.mean(values, axis=-1, keepdims=True)
    spread = jnp.mean(jnp.square(values - center), axis=-1, keepdims=True)
    return ((values - center) * lax.rsqrt(spread + 1e-05)).astype(jnp.bfloat16)


def pieces_of(size, unit, most):
    for count in range(most, 1, -1):
        if size % (count * unit) == 0:
            return count
    return 1


def hand_over(dims, cuts, up_ref, down_ref, got_up, got_down, up_room, down_room, up_sems, down_sems, room_sem):
    groups, fs, tp = dims
    pairs = tp // CORES
    up_cuts, down_cuts = cuts
    y, f, t = lax.axis_index("grp"), lax.axis_index("fs"), lax.axis_index("tp")
    x, k = t // CORES, t % CORES
    blocks = up_ref.shape[0]
    first_send, first_recv, x_send, y_send, y_recv, a_send, a_recv, b_send, b_recv = up_sems
    own_send, own_recv, dx_send, dx_recv, dy_send, dy_recv, da_send, da_recv, db_send, db_recv = down_sems
    cols = up_ref.shape[3] // up_cuts
    home = (f // blocks) // CORES
    sibling = (y, f, x * CORES + (1 - k))

    def remote(src, dst, send, recv, where):
        return pltpu.make_async_remote_copy(src_ref=src, dst_ref=dst, send_sem=send, recv_sem=recv, device_id=where, device_id_type=MESH)

    height = down_ref.shape[0] // (groups * down_cuts)
    width = down_ref.shape[1]

    def down_at(ref, group, cut, column):
        return ref.at[pl.ds(pl.multiple_of((group * down_cuts + cut) * height, height), height), pl.ds(pl.multiple_of(column * width, width), width)]

    def down_first(dx, cut):
        xo = (x + dx) % pairs
        return remote(down_at(down_ref, y, cut, 0), down_at(got_down, y, cut, t), dx_send.at[dx - 1, cut], dx_recv.at[dx - 1, cut], (y, f, xo * CORES + k))

    def down_y(dx, dy, cut):
        column = ((x - dx + pairs) % pairs) * CORES + k
        here = down_at(got_down, y, cut, column)
        return remote(here, here, dy_send.at[dx - 1, dy - 1, cut], dy_recv.at[dx - 1, dy - 1, cut], ((y + dy) % groups, f, t))

    def down_a(dx, cut):
        column = ((x - dx + pairs) % pairs) * CORES + k
        here = down_at(got_down, y, cut, column)
        return remote(here, here, da_send.at[dx - 1, cut], da_recv.at[dx - 1, cut], sibling)

    def down_b(dx, dy, cut):
        column = ((x - dx + pairs) % pairs) * CORES + k
        here = down_at(got_down, (y - dy + groups) % groups, cut, column)
        return remote(here, here, db_send.at[dx - 1, dy - 1, cut], db_recv.at[dx - 1, dy - 1, cut], sibling)

    own_columns = got_down.at[:, pl.ds(pl.multiple_of(t * width, width), width)]
    down_own = remote(down_ref, own_columns, own_send, own_recv, sibling)

    def up_at(ref, block, group, lane, cut):
        return ref.at[block, group * CORES + lane, :, pl.ds(cut * cols, cols)]

    def up_first(block, lane, cut):
        to = t * blocks + block
        return remote(up_at(up_ref, block, y, lane, cut), up_at(got_up, f, y, lane, cut), first_send.at[block, lane, cut], first_recv.at[f, cut], (y, to, x * CORES + lane))

    def up_x(r, cut, dx):
        here = up_at(got_up, r, y, k, cut)
        return remote(here, here, x_send.at[dx - 1, r, cut], first_recv.at[r, cut], (y, f, ((x + dx) % pairs) * CORES + k))

    def up_y(r, cut, dy):
        here = up_at(got_up, r, y, k, cut)
        return remote(here, here, y_send.at[dy - 1, r, cut], y_recv.at[dy - 1, r, cut], ((y + dy) % groups, f, t))

    def up_a(r, cut):
        here = up_at(got_up, r, y, k, cut)
        return remote(here, here, a_send.at[r, cut], a_recv.at[r, cut], sibling)

    def up_b(r, cut, dy):
        here = up_at(got_up, r, (y - dy + groups) % groups, k, cut)
        return remote(here, here, b_send.at[dy - 1, r, cut], b_recv.at[dy - 1, r, cut], sibling)

    def is_self(block, lane):
        return jnp.logical_and(t * blocks + block == f, lane == k)

    room_in = pltpu.make_async_copy(up_ref.at[f % blocks, y * CORES + k], up_room, room_sem.at[0])
    down_in = pltpu.make_async_copy(down_ref, down_room, room_sem.at[1])
    down_out = pltpu.make_async_copy(down_room, own_columns, room_sem.at[2])

    def room_out(cut):
        return pltpu.make_async_copy(up_room.at[:, pl.ds(cut * cols, cols)], up_at(got_up, f, y, k, cut), first_recv.at[f, cut])

    room_in.start()
    down_in.start()
    for cut in range(down_cuts):
        for dx in range(1, pairs):
            down_first(dx, cut).start()
    for cut in range(up_cuts):
        for block in range(blocks):
            for lane in range(CORES):
                @pl.when(jnp.logical_not(is_self(block, lane)))
                def _():
                    up_first(block, lane, cut).start()
    down_own.start()
    room_in.wait()
    owner = f // blocks == t

    @pl.when(owner)
    def _():
        for cut in range(up_cuts):
            room_out(cut).start()

    down_in.wait()
    down_out.start()

    for step in range(down_cuts + LAG):
        if step < down_cuts:
            for dx in range(1, pairs):
                down_first(dx, step).wait_recv()
                for dy in range(1, groups):
                    down_y(dx, dy, step).start()
                down_a(dx, step).start()
        if step >= LAG:
            for dx in range(1, pairs):
                for dy in range(1, groups):
                    down_y(dx, dy, step - LAG).wait_recv()
                    down_b(dx, dy, step - LAG).start()

    def up_arrival(step):
        cut, r = step // fs, (f + step) % fs
        pltpu.make_async_copy(up_at(got_up, r, y, k, cut), up_at(got_up, r, y, k, cut), first_recv.at[r, cut]).wait()

        @pl.when(x == home)
        def _():
            for dx in range(1, pairs):
                up_x(r, cut, dx).start()

        for dy in range(1, groups):
            up_y(r, cut, dy).start()
        up_a(r, cut).start()

    def up_second(step):
        cut, r = step // fs, (f + step) % fs
        for dy in range(1, groups):
            up_y(r, cut, dy).wait_recv()
            up_b(r, cut, dy).start()

    for step in range(up_cuts * fs + LAG):
        if step < up_cuts * fs:
            up_arrival(step)
        if step >= LAG:
            up_second(step - LAG)

    for cut in range(up_cuts):
        for r in range(fs):
            up_a(r, cut).wait()
            for dy in range(1, groups):
                up_b(r, cut, dy).wait()
                up_y(r, cut, dy).wait_send()

            @pl.when(x == home)
            def _():
                for dx in range(1, pairs):
                    up_x(r, cut, dx).wait_send()

        for block in range(blocks):
            for lane in range(CORES):
                @pl.when(jnp.logical_not(is_self(block, lane)))
                def _():
                    up_first(block, lane, cut).wait_send()
    for cut in range(down_cuts):
        for dx in range(1, pairs):
            down_first(dx, cut).wait_send()
            down_a(dx, cut).wait()
            for dy in range(1, groups):
                down_y(dx, dy, cut).wait_send()
                down_b(dx, dy, cut).wait()
    down_own.wait()
    down_out.wait()


def gather(up_cast, down_cast, dims):
    groups, fs, tp = dims
    rows, cols = up_cast.shape[0] // (groups * CORES), up_cast.shape[1] * tp // fs
    blocks = fs // tp
    by_block = up_cast.reshape(groups * CORES, rows, blocks, cols).transpose(2, 0, 1, 3)
    height, width = down_cast.shape
    up_cuts = pieces_of(cols, 128, 4)
    down_cuts = pieces_of(height // groups, 16, 8)
    pairs = tp // CORES
    dma = pltpu.SemaphoreType.DMA
    up_sems = [
        dma((blocks, CORES, up_cuts)),
        dma((fs, up_cuts)),
        dma((pairs - 1, fs, up_cuts)),
        dma((groups - 1, fs, up_cuts)),
        dma((groups - 1, fs, up_cuts)),
        dma((fs, up_cuts)),
        dma((fs, up_cuts)),
        dma((groups - 1, fs, up_cuts)),
        dma((groups - 1, fs, up_cuts)),
    ]
    one, two = (pairs - 1, down_cuts), (pairs - 1, groups - 1, down_cuts)
    down_sems = [dma, dma, dma(one), dma(one), dma(two), dma(two), dma(one), dma(one), dma(two), dma(two)]
    got_up, got_down = pl.pallas_call(
        functools.partial(hand_over, dims, (up_cuts, down_cuts)),
        out_shape=(
            jax.ShapeDtypeStruct((fs, groups * CORES, rows, cols), jnp.bfloat16),
            jax.ShapeDtypeStruct((height, tp * width), jnp.bfloat16),
        ),
        in_specs=[pl.BlockSpec(memory_space=pl.ANY)] * 2,
        out_specs=(pl.BlockSpec(memory_space=pl.ANY),) * 2,
        scratch_shapes=[
            pltpu.VMEM((rows, cols), jnp.bfloat16),
            pltpu.VMEM((height, width), jnp.bfloat16),
            up_sems,
            down_sems,
            dma((3,)),
        ],
        compiler_params=pltpu.CompilerParams(has_side_effects=True),
    )(by_block, down_cast)
    return got_up.reshape(fs * groups * CORES * rows, cols), got_down


def shards(dims, tokens, up_master, down_master, norm_gain):
    up_cast = (norm_gain[:, None] * up_master).astype(jnp.bfloat16)
    down_cast = down_master.astype(jnp.bfloat16)
    sampled_up, sampled_down = gather(up_cast, down_cast, dims)
    normalized = normalize(tokens)
    before = jnp.dot(normalized, sampled_up, preferred_element_type=jnp.float32)
    hidden = jnp.square(jax.nn.relu(before)).astype(jnp.bfloat16)
    terms = jnp.dot(hidden, sampled_down, preferred_element_type=jnp.float32)
    summed = lax.psum_scatter(terms, "fs", scatter_dimension=1, tiled=True)
    return (summed.astype(jnp.bfloat16), sampled_up, sampled_down)


def solution(mesh):
    dims = tuple(mesh.shape[name] for name in ("grp", "fs", "tp"))
    return jax.shard_map(
        functools.partial(shards, dims),
        mesh=mesh,
        in_specs=(P(("grp", "tp"), None), P("fs", "tp"), P("fs", "tp"), P("fs")),
        out_specs=(P(("grp", "tp"), "fs"), P("grp", "fs"), P(("grp", "fs"), None)),
        check_vma=False,
    )
```

time: 525 us -> 316 us (0.60)
  waiting for transfers between devices: 283 us -> 59.7 us
  Pallas kernels: 0 us -> 181 us
  blocking collectives: 164 us -> 0 us
    all_gather x2 -> x0, waiting for transfers between devices: 223 us -> none  [the longest x1 113 us: shards(): lax.all_gather(down_cast, 'tp', axis=1, tiled=True)]
    pallas_call x0 -> x1, Pallas kernels: none -> 181 us  [gather(): pl.pallas_call(functools.partial(hand_over, dims, (up_cuts, down_cuts)),...]
    all_to_all x2 -> x0, blocking collectives: 164 us -> none  [the longest x1 108 us: shards(): lax.all_to_all(quarter, 'fs', split_axis=1, concat_axis=0, tiled=True)]
    unnamed x14 -> x20, local copies, waits for them, and re-layouts: 27.6 us -> 29 us
  transfers between devices with their start and end apart: 3 -> 1, of which waited for: 3 -> 1; matrix products, arithmetic and copies ran while one was open for 3% -> 0% of each run, Pallas kernels for 0% -> 0%
where the time goes in v1:
time: 316 us; the launch traced here: 314 us
  Pallas kernels  181 us (57%)
  waiting for transfers between devices  59.7 us (19%)
  local copies, waits for them, and re-layouts  29 us (9%)
  matrix products  16.4 us (5%)
  between operations  14.1 us (4%)
  other arithmetic  13.4 us (4%)
    pallas_call x1, Pallas kernels, gather(): pl.pallas_call(functools.partial(hand_over, dims, (up_cuts, down_cuts)),...  181 us
    reduce_scatter x1, waiting for transfers between devices, shards(): summed = lax.psum_scatter(terms, 'fs', scatter_dimension=1, tiled=True)  59.7 us
    unnamed x20, local copies, waits for them, and re-layouts  29 us
    dot_general x1, matrix products, shards(): before = jnp.dot(normalized, sampled_up, preferred_element_type=jnp.float32)  9.59 us
    dot_general x1, matrix products, shards(): terms = jnp.dot(hidden, sampled_down, preferred_element_type=jnp.float32)  6.86 us
    convert_element_type x1, other arithmetic, shards(): down_cast = down_master.astype(jnp.bfloat16)  6.69 us
  transfers between devices with their start and end apart: 1, of which 1 were waited for; matrix products, arithmetic and copies ran while one was open for 0% of the time, Pallas kernels for 0%

profile of v1, /device:TPU:3, one launch (start us, length us, event | category | flops | bytes accessed | tf_op | source)
XLA Modules:
  0.0 313.7 jit_solution(1022735186836176143)
XLA Ops:
  7.2 0.0 copy-start.2
  7.2 0.0 reduce-scatter.2.cloned.1.call-start
  7.2 0.0 copy-start.1
  7.2 6.7 %convert_element_type.21.down_ref = bf16[3072,768]{1,0:T(8,128)(2,1)} convert(f32[3072,768]{1,0:T(8,128)} %param.6) | non-fusion elementwise | flops 2359296 | bytes 14155776 | tf_op jit(solution)/shard_map/convert_element_type | solution.py:240
  13.9 0.0 copy-done.2
  13.9 0.0 copy-start.3
  13.9 0.3 convert_reduce_fusion
  14.2 0.6 fusion.4
  14.8 0.9 copy-done.1
  15.7 0.0 copy-done.3
  15.7 3.8 %multiply_convert_fusion = bf16[768,3072]{1,0:T(8,128)(2,1)} fusion(f32[768,3072]{1,0:T(8,128)S(1)} %copy-done.1, f32[768]{0:T(1024)S(1)} %copy-done.3), kind=kLoop, calls=%fused_computation | loop fusion | flops 4718592 | bytes 14158848 | tf_op jit(solution)/shard_map/convert_element_type | solution.py:239
  19.5 181.0 %shard_map.67 = (bf16[4,4,192,3072]{3,2,1,0:T(8,128)(2,1)}, bf16[3072,3072]{1,0:T(8,128)(2,1)}) custom-call(bf16[1,4,192,3072]{3,2,1,0:T(8,128)(2,1)} %bitcast.9, bf16[3072,768]{1,0:T(8,128)(2,1)} %convert_element_type.21.down_ref), custom_call_target="tpu_custom_call" | custom-call | tf_op jit(solution)/shard_map/pallas_call | solution.py:218
  200.5 0.0 copy-start
  200.5 9.6 %fusion.1 = bf16[256,3072]{1,0:T(8,128)(2,1)S(1)} fusion(bf16[3072,3072]{1,0:T(8,128)(2,1)} %bitcast.7, bf16[256,3072]{1,0:T(8,128)(2,1)S(1)} %copy-done.2, f32[256]{0:T(256)S(1)} %add_rsqrt_fusion, f32[256]{0:T(256)S(1)} %broadcast_multiply_fusion), kind=kOutput, calls=%fused_computation.5 | convolution fusion | flops 4837343232 | bytes 22022144 | tf_op jit(solution)/shard_map/dot_general | solution.py:243
  210.1 2.1 copy-done
  212.2 6.9 %fusion.9 = f32[256,3072]{1,0:T(8,128)} fusion(bf16[256,3072]{1,0:T(8,128)(2,1)S(1)} %fusion.1, bf16[3072,3072]{1,0:T(8,128)(2,1)S(1)} %copy-done), kind=kOutput, calls=%fused_computation.14 | convolution fusion | flops 4831838208 | bytes 23592960 | tf_op jit(solution)/shard_map/dot_general | solution.py:245
  219.1 0.0 reduce-scatter.2.cloned.1.call-update
  219.1 59.7 %reduce-scatter.2.cloned.1.call-done = f32[256,768]{1,0:T(8,128)} async-done(((f32[256,3072]{1,0:T(8,128)}), f32[256,768]{1,0:T(8,128)}) %reduce-scatter.2.cloned.1.call-update) | async-done | bytes 786448 | tf_op jit(solution)/shard_map/reduce_scatter | solution.py:246
  278.8 0.0 slice-start
  278.8 2.1 convert_element_type.23
  280.8 0.0 slice-start.1
  280.8 0.0 slice-start.2
  280.8 0.0 slice-start.3
  280.8 0.0 slice-start.4
  280.8 19.1 %copy.9 = bf16[3072,3072]{1,0:T(8,128)(2,1)} copy(bf16[3072,3072]{1,0:T(8,128)(2,1)} %bitcast.8) | data formatting | bytes 37748736
  299.9 0.0 slice-done
  299.9 0.0 slice-done.1
  299.9 0.0 slice-done.2
  299.9 0.0 slice-done.3
  300.0 0.0 slice-done.4
  300.0 6.9 %copy.10 = bf16[3072,3072]{1,0:T(8,128)(2,1)} copy(bf16[3072,3072]{1,0:T(8,128)(2,1)S(1)} %bitcast.6) | data formatting | bytes 37748736
  (3 shorter events, 0.0 us)
Async XLA Ops:
  7.2 6.8 %copy-start.2 = (bf16[256,3072]{1,0:T(8,128)(2,1)S(1)}, bf16[256,3072]{1,0:T(8,128)(2,1)}, u32[]{:S(2)}) copy-start(bf16[256,3072]{1,0:T(8,128)(2,1)} %param.4) | copy-start | bytes 4718596
  7.2 271.6 %reduce-scatter.2.cloned.1.call-start = ((), (), s32[]{:S(2)}) async-start(), calls=%async_computation.1 | async-start | bytes 3932160 | tf_op jit(solution)/shard_map/reduce_scatter | solution.py:246
  7.2 8.5 %copy-start.1 = (f32[768,3072]{1,0:T(8,128)S(1)}, f32[768,3072]{1,0:T(8,128)}, u32[]{:S(2)}) copy-start(f32[768,3072]{1,0:T(8,128)} %param.5) | copy-start | bytes 28311556
  13.9 1.8 copy-start.3
  200.5 11.7 %copy-start = (bf16[3072,3072]{1,0:T(8,128)(2,1)S(1)}, bf16[3072,3072]{1,0:T(8,128)(2,1)}, u32[]{:S(2)}) copy-start(bf16[3072,3072]{1,0:T(8,128)(2,1)} %get-tuple-element.12) | copy-start | bytes 56623108
  278.8 21.2 %slice-start = ((s8[18874368]{0:T(1024)(128)(4,1)}), s8[4194304]{0:T(1024)(128)(4,1)S(1)}, s32[]{:S(2)}) async-start(s8[18874368]{0:T(1024)(128)(4,1)} %bitcast.5), calls=%async_computation.2 | async-start | bytes 8388608
  280.8 19.1 %slice-start.1 = ((s8[18874368]{0:T(1024)(128)(4,1)}), s8[4194304]{0:T(1024)(128)(4,1)S(1)}, s32[]{:S(2)}) async-start(s8[18874368]{0:T(1024)(128)(4,1)} %bitcast.5), calls=%async_computation.3 | async-start | bytes 8388608
  280.8 19.1 %slice-start.2 = ((s8[18874368]{0:T(1024)(128)(4,1)}), s8[4194304]{0:T(1024)(128)(4,1)S(1)}, s32[]{:S(2)}) async-start(s8[18874368]{0:T(1024)(128)(4,1)} %bitcast.5), calls=%async_computation.4 | async-start | bytes 8388608
  280.8 19.1 %slice-start.3 = ((s8[18874368]{0:T(1024)(128)(4,1)}), s8[4194304]{0:T(1024)(128)(4,1)S(1)}, s32[]{:S(2)}) async-start(s8[18874368]{0:T(1024)(128)(4,1)} %bitcast.5), calls=%async_computation.5 | async-start | bytes 8388608
  280.8 19.1 %slice-start.4 = ((s8[18874368]{0:T(1024)(128)(4,1)}), s8[2097152]{0:T(1024)(128)(4,1)S(1)}, s32[]{:S(2)}) async-start(s8[18874368]{0:T(1024)(128)(4,1)} %bitcast.5), calls=%async_computation.6 | async-start | bytes 4194304
Sparse Core Ops, SparseCore 0:
  219.2 59.5 reduce-scatter.1

commit v2 on v0

v2 whole, which is shorter than its diff:
```python
import functools

import jax
import jax.numpy as jnp
from jax import lax
from jax.experimental import pallas as pl
from jax.experimental.pallas import tpu as pltpu
from jax.sharding import PartitionSpec as P

MESH = pl.DeviceIdType.MESH
CORES = 2
LAG = 2
EARLY = 2
UNIT = 256
LIMIT = 14


def normalize(tokens):
    values = tokens.astype(jnp.float32)
    center = jnp.mean(values, axis=-1, keepdims=True)
    spread = jnp.mean(jnp.square(values - center), axis=-1, keepdims=True)
    return ((values - center) * lax.rsqrt(spread + 1e-05)).astype(jnp.bfloat16)


def pieces_of(size, unit, most):
    for count in range(most, 1, -1):
        if size % (count * unit) == 0:
            return count
    return 1


def hand_over(dims, cuts, rows_ref, up_ref, down_ref, got_up, got_down, out_ref, hidden, mine, sent, landed, up_sems, down_sems, sum_sems, local_sem):
    groups, fs, tp = dims
    pairs = tp // CORES
    up_cuts, down_cuts = cuts
    y, f, t = lax.axis_index("grp"), lax.axis_index("fs"), lax.axis_index("tp")
    x, k = t // CORES, t % CORES
    first_send, first_recv, x_send, y_send, y_recv, a_send, a_recv, b_send, b_recv = up_sems
    own_send, own_recv, dx_send, dx_recv, dy_send, dy_recv, da_send, da_recv, db_send, db_recv = down_sems
    sum_send, sum_recv = sum_sems
    cols = up_ref.shape[2] // up_cuts
    depth = got_up.shape[0] * got_up.shape[1] * got_up.shape[2]
    home = f // CORES
    sibling = (y, f, x * CORES + (1 - k))

    def remote(src, dst, send, recv, where):
        return pltpu.make_async_remote_copy(src_ref=src, dst_ref=dst, send_sem=send, recv_sem=recv, device_id=where, device_id_type=MESH)

    height = down_ref.shape[0] // groups
    width = down_ref.shape[1]
    tile = width // down_cuts

    def down_at(ref, group, cut, column):
        return ref.at[pl.ds(pl.multiple_of(group * height, height), height), pl.ds(pl.multiple_of(column * width + cut * tile, tile), tile)]

    def from_pair(dx):
        return ((x - dx + pairs) % pairs) * CORES + k

    def down_first(dx, cut):
        return remote(down_at(down_ref, y, cut, 0), down_at(got_down, y, cut, t), dx_send.at[dx - 1, cut], dx_recv.at[dx - 1, cut], (y, f, ((x + dx) % pairs) * CORES + k))

    def down_y(dx, dy, cut):
        here = down_at(got_down, y, cut, from_pair(dx))
        return remote(here, here, dy_send.at[dx - 1, dy - 1, cut], dy_recv.at[dx - 1, dy - 1, cut], ((y + dy) % groups, f, t))

    def down_a(dx, cut):
        here = down_at(got_down, y, cut, from_pair(dx))
        return remote(here, here, da_send.at[dx - 1, cut], da_recv.at[dx - 1, cut], sibling)

    def down_b(dx, dy, cut):
        here = down_at(got_down, (y - dy + groups) % groups, cut, from_pair(dx))
        return remote(here, here, db_send.at[dx - 1, dy - 1, cut], db_recv.at[dx - 1, dy - 1, cut], sibling)

    own_columns = got_down.at[:, pl.ds(pl.multiple_of(t * width, width), width)]
    down_own = remote(down_ref, own_columns, own_send, own_recv, sibling)
    down_here = pltpu.make_async_copy(down_ref, own_columns, local_sem)

    def up_at(ref, group, lane, cut):
        return ref.at[group * CORES + lane, :, pl.ds(cut * cols, cols)]

    def up_first(lane, cut):
        return remote(up_at(up_ref, y, lane, cut), up_at(got_up.at[f], y, lane, cut), first_send.at[lane, cut], first_recv.at[f, cut], (y, t, x * CORES + lane))

    def up_here(r, cut):
        return pltpu.make_async_copy(up_at(up_ref, y, k, cut), up_at(got_up.at[r], y, k, cut), first_recv.at[r, cut])

    def up_x(r, cut, dx):
        here = up_at(got_up.at[r], y, k, cut)
        return remote(here, here, x_send.at[dx - 1, r, cut], first_recv.at[r, cut], (y, f, ((x + dx) % pairs) * CORES + k))

    def up_y(r, cut, dy):
        here = up_at(got_up.at[r], y, k, cut)
        return remote(here, here, y_send.at[dy - 1, r, cut], y_recv.at[dy - 1, r, cut], ((y + dy) % groups, f, t))

    def up_a(r, cut):
        here = up_at(got_up.at[r], y, k, cut)
        return remote(here, here, a_send.at[r, cut], a_recv.at[r, cut], sibling)

    def up_b(r, cut, dy):
        here = up_at(got_up.at[r], (y - dy + groups) % groups, k, cut)
        return remote(here, here, b_send.at[dy - 1, r, cut], b_recv.at[dy - 1, r, cut], sibling)

    def is_self(lane):
        return jnp.logical_and(t == f, lane == k)

    def hidden_units(cut):
        @pl.loop(0, cols // UNIT)
        def _(step):
            at = pl.ds(pl.multiple_of(cut * cols + step * UNIT, UNIT), UNIT)
            block = got_up[:, :, :, at].reshape(depth, UNIT)
            before = jnp.dot(rows_ref[...], block, preferred_element_type=jnp.float32)
            hidden[:, at] = jnp.square(jnp.maximum(before, 0.0)).astype(jnp.bfloat16)

    def sum_to(column, cut):
        at = pl.ds(cut * tile, tile)
        return remote(sent.at[column, :, at], landed.at[f, :, at], sum_send.at[column, cut], sum_recv.at[f, cut], (y, column, t))

    def features(column, cut):
        at = pl.ds(pl.multiple_of(column * width + cut * tile, tile), tile)
        term = jnp.dot(hidden[...], got_down[:, at], preferred_element_type=jnp.float32)

        @pl.when(column == f)
        def _():
            mine[:, pl.ds(cut * tile, tile)] = term

        @pl.when(column != f)
        def _():
            sent[column, :, pl.ds(cut * tile, tile)] = term.astype(jnp.bfloat16)
            sum_to(column, cut).start()

    early = min(EARLY, down_cuts)
    for lane in range(CORES):
        @pl.when(is_self(lane))
        def _():
            for cut in range(up_cuts):
                up_here(f, cut).start()
    for cut in range(early):
        for dx in range(1, pairs):
            down_first(dx, cut).start()
    for cut in range(up_cuts):
        for lane in range(CORES):
            @pl.when(jnp.logical_not(is_self(lane)))
            def _():
                up_first(lane, cut).start()
    down_here.start()
    down_own.start()

    @pl.when(x != home)
    def _():
        for cut in range(early, down_cuts):
            for dx in range(1, pairs):
                down_first(dx, cut).start()

    order = [(0, cut) for cut in range(up_cuts)] + [(j, cut) for cut in range(up_cuts) for j in range(1, fs)]

    def up_arrival(j, cut):
        r = (f + j) % fs
        up_here(r, cut).wait()

        @pl.when(x == home)
        def _():
            for dx in range(1, pairs):
                up_x(r, cut, dx).start()

        for dy in range(1, groups):
            up_y(r, cut, dy).start()
        up_a(r, cut).start()

    def up_second(j, cut):
        r = (f + j) % fs
        for dy in range(1, groups):
            up_y(r, cut, dy).wait_recv()
            up_b(r, cut, dy).start()

    def up_done(cut):
        for j in range(fs):
            r = (f + j) % fs
            up_a(r, cut).wait_recv()
            for dy in range(1, groups):
                up_b(r, cut, dy).wait_recv()
        hidden_units(cut)

    done = 0
    for step in range(len(order) + LAG):
        if step < len(order):
            up_arrival(*order[step])
        if step == len(order) - 1:
            @pl.when(x == home)
            def _():
                for cut in range(early, down_cuts):
                    for dx in range(1, pairs):
                        down_first(dx, cut).start()
        if step >= LAG:
            up_second(*order[step - LAG])
        if done < up_cuts - 1 and step == up_cuts + (done + 2) * (fs - 1) - 1:
            up_done(done)
            done += 1

    down_here.wait()
    for step in range(down_cuts + 2):
        if step < down_cuts:
            for dx in range(1, pairs):
                down_first(dx, step).wait_recv()
                for dy in range(1, groups):
                    down_y(dx, dy, step).start()
                down_a(dx, step).start()
        if step == 0:
            for cut in range(done, up_cuts):
                up_done(cut)
        if 1 <= step <= down_cuts:
            for dx in range(1, pairs):
                for dy in range(1, groups):
                    down_y(dx, dy, step - 1).wait_recv()
                    down_b(dx, dy, step - 1).start()
        if step < down_cuts:
            features(t, step)
            if step == 0:
                down_own.wait_recv()
            features(x * CORES + (1 - k), step)
        if 1 <= step <= down_cuts:
            for dx in range(1, pairs):
                features(from_pair(dx), step - 1)
        if step >= 2:
            for dx in range(1, pairs):
                down_a(dx, step - 2).wait_recv()
                for dy in range(1, groups):
                    down_b(dx, dy, step - 2).wait_recv()
                features(((x - dx + pairs) % pairs) * CORES + (1 - k), step - 2)

    for cut in range(down_cuts):
        at = pl.ds(cut * tile, tile)
        for j in range(1, fs):
            r = (f + j) % fs
            remote(sent.at[r, :, at], landed.at[r, :, at], sum_send.at[r, cut], sum_recv.at[r, cut], (y, r, t)).wait_recv()
        total = mine[:, at]
        for j in range(1, fs):
            total += landed[(f + j) % fs, :, at].astype(jnp.float32)
        out_ref[:, at] = total.astype(jnp.bfloat16)

    for cut in range(up_cuts):
        for j in range(fs):
            r = (f + j) % fs
            up_a(r, cut).wait_send()
            for dy in range(1, groups):
                up_b(r, cut, dy).wait_send()
                up_y(r, cut, dy).wait_send()

            @pl.when(x == home)
            def _():
                for dx in range(1, pairs):
                    up_x(r, cut, dx).wait_send()

        for lane in range(CORES):
            @pl.when(jnp.logical_not(is_self(lane)))
            def _():
                up_first(lane, cut).wait_send()
    for cut in range(down_cuts):
        for dx in range(1, pairs):
            down_first(dx, cut).wait_send()
            down_a(dx, cut).wait_send()
            for dy in range(1, groups):
                down_y(dx, dy, cut).wait_send()
                down_b(dx, dy, cut).wait_send()
        for j in range(1, fs):
            sum_to((f + j) % fs, cut).wait_send()
    down_own.wait_send()


def fused(rows_in, up_cast, down_cast, dims):
    groups, fs, tp = dims
    rows, cols = up_cast.shape[0] // (groups * CORES), up_cast.shape[1]
    height, width = down_cast.shape
    tokens = rows_in.shape[0]
    up_cuts = pieces_of(cols, UNIT, 4)
    down_cuts = pieces_of(width, 128, 6)
    pairs = tp // CORES
    dma = pltpu.SemaphoreType.DMA
    far = groups - 1
    up_sems = [dma((CORES, up_cuts)), dma((fs, up_cuts)), dma((pairs - 1, fs, up_cuts)), dma((far, fs, up_cuts)), dma((far, fs, up_cuts))]
    up_sems += [dma((fs, up_cuts)), dma((fs, up_cuts)), dma((far, fs, up_cuts)), dma((far, fs, up_cuts))]
    one, two = (pairs - 1, down_cuts), (pairs - 1, far, down_cuts)
    down_sems = [dma, dma, dma(one), dma(one), dma(two), dma(two), dma(one), dma(one), dma(two), dma(two)]
    vmem = pl.BlockSpec(memory_space=pltpu.VMEM)
    hbm = pl.BlockSpec(memory_space=pl.ANY)
    got_up, got_down, out = pl.pallas_call(
        functools.partial(hand_over, dims, (up_cuts, down_cuts)),
        out_shape=(
            pltpu.VMEM((fs, groups * CORES, rows, cols), jnp.bfloat16),
            pltpu.VMEM((height, tp * width), jnp.bfloat16),
            jax.ShapeDtypeStruct((tokens, width), jnp.bfloat16),
        ),
        in_specs=[vmem, hbm, hbm],
        out_specs=(vmem, vmem, vmem),
        scratch_shapes=[
            pltpu.VMEM((tokens, cols), jnp.bfloat16),
            pltpu.VMEM((tokens, width), jnp.float32),
            pltpu.VMEM((fs, tokens, width), jnp.bfloat16),
            pltpu.VMEM((fs, tokens, width), jnp.bfloat16),
            up_sems,
            down_sems,
            [dma((fs, down_cuts)), dma((fs, down_cuts))],
            dma,
        ],
        compiler_params=pltpu.CompilerParams(has_side_effects=True, vmem_limit_bytes=LIMIT << 20),
    )(rows_in, up_cast.reshape(groups * CORES, rows, cols), down_cast)
    return out, got_up.reshape(fs * groups * CORES * rows, cols), got_down


def fits(up_shape, down_shape, dims):
    groups, fs, tp = dims
    own = 2 * (up_shape[0] * up_shape[1] * fs + down_shape[0] * down_shape[1] * tp)
    aligned = up_shape[0] % (groups * CORES * 16) == 0 and up_shape[1] % UNIT == 0
    return fs == tp and groups > 1 and tp % CORES == 0 and tp > CORES and aligned and down_shape[0] % (groups * 16) == 0 and down_shape[1] % 128 == 0 and own <= 40 << 20


def by_collectives(normalized, up_cast, down_cast):
    quarter = lax.all_to_all(up_cast, "tp", split_axis=0, concat_axis=1, tiled=True)
    moved = lax.all_to_all(quarter, "fs", split_axis=1, concat_axis=0, tiled=True)
    part_rows = quarter.shape[0]
    stacked = moved.reshape(moved.shape[0] // part_rows, part_rows, moved.shape[1])
    joined = lax.all_gather(stacked, "tp", axis=1, tiled=True)
    sampled_down = lax.all_gather(down_cast, "tp", axis=1, tiled=True)
    sampled_up = joined.reshape(joined.shape[0] * joined.shape[1], joined.shape[2])
    before = jnp.dot(normalized, sampled_up, preferred_element_type=jnp.float32)
    hidden = jnp.square(jax.nn.relu(before)).astype(jnp.bfloat16)
    terms = jnp.dot(hidden, sampled_down, preferred_element_type=jnp.float32)
    summed = lax.psum_scatter(terms, "fs", scatter_dimension=1, tiled=True)
    return summed.astype(jnp.bfloat16), sampled_up, sampled_down


def shards(dims, tokens, up_master, down_master, norm_gain):
    up_cast = (norm_gain[:, None] * up_master).astype(jnp.bfloat16)
    down_cast = down_master.astype(jnp.bfloat16)
    normalized = normalize(tokens)
    if fits(up_master.shape, down_master.shape, dims):
        return fused(normalized, up_cast, down_cast, dims)
    return by_collectives(normalized, up_cast, down_cast)


def solution(mesh):
    dims = tuple(mesh.shape[name] for name in ("grp", "fs", "tp"))
    return jax.shard_map(
        functools.partial(shards, dims),
        mesh=mesh,
        in_specs=(P(("grp", "tp"), None), P("fs", "tp"), P("fs", "tp"), P("fs")),
        out_specs=(P(("grp", "tp"), "fs"), P("grp", "fs"), P(("grp", "fs"), None)),
        check_vma=False,
    )
```

time: 525 us -> 246 us (0.47)
  waiting for transfers between devices: 283 us -> 0 us
  Pallas kernels: 0 us -> 212 us
  blocking collectives: 164 us -> 0 us
  matrix products: 20.1 us -> 0 us
  between operations: 13.8 us -> 0.69 us
  local copies, waits for them, and re-layouts: 27.6 us -> 14.5 us
    all_gather x2 -> x0, waiting for transfers between devices: 223 us -> none  [the longest x1 113 us: shards(): lax.all_gather(down_cast, 'tp', axis=1, tiled=True)]
    pallas_call x0 -> x1, Pallas kernels: none -> 212 us  [fused(): pl.pallas_call(functools.partial(hand_over, dims, (up_cuts, down_cuts)),...]
    all_to_all x2 -> x0, blocking collectives: 164 us -> none  [the longest x1 108 us: shards(): lax.all_to_all(quarter, 'fs', split_axis=1, concat_axis=0, tiled=True)]
    reduce_scatter x1 -> x0, waiting for transfers between devices: 60.9 us -> none  [shards(): summed = lax.psum_scatter(terms, 'fs', scatter_dimension=1, tiled=True)]
    dot_general x2 -> x0, matrix products: 20.1 us -> none  [the longest x1 10.7 us: shards(): terms = jnp.dot(hidden, sampled_down, preferred_element_type=jnp.float32)]
    unnamed x14 -> x7, local copies, waits for them, and re-layouts: 27.6 us -> 14.5 us
  transfers between devices with their start and end apart: 3 -> 0, of which waited for: 3 -> 0; matrix products, arithmetic and copies ran while one was open for 3% -> 0% of each run, Pallas kernels for 0% -> 0%
where the time goes in v2:
time: 246 us
  Pallas kernels  212 us (86%)
  other arithmetic  18 us (7%)
  local copies, waits for them, and re-layouts  14.5 us (6%)
    pallas_call x1, Pallas kernels, fused(): pl.pallas_call(functools.partial(hand_over, dims, (up_cuts, down_cuts)),...  212 us
    unnamed x7, local copies, waits for them, and re-layouts  14.5 us
    convert_element_type x1, other arithmetic, shards(): up_cast = (norm_gain[:, None] * up_master).astype(jnp.bfloat16)  7.3 us
    convert_element_type x1, other arithmetic, shards(): down_cast = down_master.astype(jnp.bfloat16)  6.32 us

profile of v2, /device:TPU:3, one launch (start us, length us, event | category | flops | bytes accessed | tf_op | source)
XLA Modules:
  0.0 245.6 jit_solution(8220297463837462955)
XLA Ops:
  0.6 0.0 copy-start
  0.6 0.0 copy-start.1
  0.7 1.8 convert_reduce_fusion
  2.5 2.0 fusion.2
  4.4 0.0 copy-done
  4.5 0.6 fusion.3.rows_ref
  5.1 0.0 copy-done.1
  5.1 7.3 %multiply_convert_fusion = bf16[768,3072]{1,0:T(8,128)(2,1)} fusion(f32[768,3072]{1,0:T(8,128)} %param.5, f32[768]{0:T(1024)S(1)} %copy-done.1), kind=kLoop, calls=%fused_computation | loop fusion | flops 4718592 | bytes 14158848 | tf_op jit(solution)/shard_map/convert_element_type | solution.py:332
  12.4 6.3 %convert_element_type.15.down_ref = bf16[3072,768]{1,0:T(8,128)(2,1)} convert(f32[3072,768]{1,0:T(8,128)} %param.6) | non-fusion elementwise | flops 2359296 | bytes 14155776 | tf_op jit(solution)/shard_map/convert_element_type | solution.py:333
  18.7 212.4 %shard_map.67 = (bf16[4,4,192,3072]{3,2,1,0:T(8,128)(2,1)S(1)}, bf16[3072,3072]{1,0:T(8,128)(2,1)S(1)}, bf16[256,768]{1,0:T(8,128)(2,1)S(1)}) custom-call(bf16[256,3072]{1,0:T(8,128)(2,1)S(1)} %fusion.3.rows_ref, bf16[4,192,3072]{2,1,0:T(8,128)(2,1)} %bitcast.3, bf16[3072,768]{1,0:T(8,128)(2,1)} %convert_element_type.15.down_ref), custom_call_target="tpu_custom_call" | custom-call | tf_op jit(solution)/shard_map/pallas_call | solution.py:285
  231.1 6.9 %copy.10 = bf16[3072,3072]{1,0:T(8,128)(2,1)} copy(bf16[3072,3072]{1,0:T(8,128)(2,1)S(1)} %bitcast.2) | data formatting | bytes 37748736
  238.0 6.8 %copy.11 = bf16[3072,3072]{1,0:T(8,128)(2,1)} copy(bf16[3072,3072]{1,0:T(8,128)(2,1)S(1)} %get-tuple-element.11) | data formatting | bytes 37748736
  244.8 0.7 copy.12
  (2 shorter events, 0.0 us)
Async XLA Ops:
  0.6 3.8 %copy-start = (bf16[256,3072]{1,0:T(8,128)(2,1)S(1)}, bf16[256,3072]{1,0:T(8,128)(2,1)}, u32[]{:S(2)}) copy-start(bf16[256,3072]{1,0:T(8,128)(2,1)} %param.4) | copy-start | bytes 4718596
  0.6 4.5 %copy-start.1 = (f32[768]{0:T(1024)S(1)}, f32[768]{0:T(1024)}, u32[]{:S(2)}) copy-start(f32[768]{0:T(1024)} %param.7) | copy-start | bytes 9220
